TPU v7x, 128 devices: a whole 4x4x4 slice. The times are simulated.
128 devices in a mesh: sp: 64 (over z, y, x), tp: 2 (over core).
Axes of the slice: x: 4, y: 4, z: 4, core: 2. Of those that a mesh axis runs over, the one named last changes fastest.
Arguments:
- stream: bfloat16 [16384, 2048], P(('sp', 'tp')), may hold values from -6 to 6
- outer_gate: bfloat16 [16384, 1024], P('sp', 'tp'), may hold values from -6 to 6
- inner_gate: bfloat16 [16384, 1024], P('sp', 'tp'), may hold values from -6 to 6
- conv_values: bfloat16 [16384, 1024], P('sp', 'tp'), may hold values from -6 to 6
- doc_ids: int32 [16384], P('sp'), may hold values from 0 to 31, never falling along the last dimension, each value on 1 to 1024 neighbouring positions
- conv_taps: float32 [3, 1024], P(None, 'tp'), may hold values from -3.5 to 3.5
- out_weight: bfloat16 [1024, 2048], replicated, may hold values from -0.1875 to 0.1875
- norm_gain: float32 [2048], replicated, may hold values from 0.1 to 1.9
- route_ids: int32 [16384, 2], P(('sp', 'tp')), may hold values from 0 to 127, all different within a row; in each aligned block of 128 rows (0 to 127, 128 to 255, ...) at most 4 rows name the same one
- route_logits: float32 [16384, 2], P(('sp', 'tp')), may hold values from -4 to 4
- group_weight: float32 [16384], P(('sp', 'tp')), may hold values from 0.25 to 1
- w_gate: bfloat16 [128, 2048, 1024], P(('sp', 'tp')), may hold values from -0.125 to 0.125
- w_up: bfloat16 [128, 2048, 1024], P(('sp', 'tp')), may hold values from -0.125 to 0.125
- w_down: bfloat16 [128, 1024, 2048], P(('sp', 'tp')), may hold values from -0.1875 to 0.1875
Outputs:
- result: bfloat16 [16384, 2048], P(('sp', 'tp'))
Inputs may be any that keep to these rules, and one draw needn't show every extreme that they name: `route_ids`: the two experts of a token differ. In the rows of one device (aligned blocks of 128 rows) no expert is named more than 4 times, a bound that some block reaches. `doc_ids`: document numbers never fall along the sequence; a document has 1 to 1024 positions and one has exactly 1024.
All inputs are finite; a program needn't handle non-finite values.
Results may differ from a plain program's by a relative error of at most 0.0052.
Values may be sent and summed in bfloat16 or wider, within the bound.
A program may use at most 64 MiB of HBM per device.

v0:
```python
import jax
import jax.numpy as jnp
from jax import lax
from jax.sharding import PartitionSpec as P


def padded_2(shard, sides, width):
    for axis, dim in sides:
        size, length = (lax.axis_size(axis), shard.shape[dim])
        up = [(i, (i + 1) % size) for i in range(size - 1)]
        down = [(j, i) for i, j in up]
        last = lax.slice_in_dim(shard, length - width, length, axis=dim)
        leading = lax.slice_in_dim(shard, 0, width, axis=dim)
        before = lax.ppermute(last, axis, up)
        after = lax.ppermute(leading, axis, down)
        shard = jnp.concatenate([before, shard, after], axis=dim)
    return shard


def on_device(
    stream,
    outer_gate,
    inner_gate,
    conv_values,
    doc_ids,
    conv_taps,
    out_weight,
    norm_gain,
    route_ids,
    route_logits,
    group_weight,
    w_gate,
    w_up,
    w_down,
):
    tok_rows = stream.shape[0]
    width = stream.shape[1]
    product = (inner_gate.astype(jnp.float32) * conv_values.astype(jnp.float32)).astype(
        jnp.bfloat16
    )
    doc_float = doc_ids.astype(jnp.bfloat16)
    padded, padded_docs = (padded_2(product, (("sp", 0),), 1), padded_2(doc_float, (("sp", 0),), 1))
    same_prev = (padded_docs[:-2] == doc_float).astype(jnp.float32)[:, None]
    same_next = (padded_docs[2:] == doc_float).astype(jnp.float32)[:, None]
    conv = (
        conv_taps[0] * padded[:-2].astype(jnp.float32) * same_prev
        + conv_taps[1] * product.astype(jnp.float32)
        + conv_taps[2] * padded[2:].astype(jnp.float32) * same_next
    )
    mixed = (outer_gate.astype(jnp.float32) * conv).astype(jnp.bfloat16)
    channels = lax.all_to_all(mixed, "tp", split_axis=0, concat_axis=1, tiled=True)
    projected = jnp.dot(channels, out_weight, preferred_element_type=jnp.float32)
    resid = stream.astype(jnp.float32) + projected
    scale = lax.rsqrt(jnp.mean(resid * resid, axis=-1, keepdims=True) + 1e-06)
    normed = (resid * scale * norm_gain).astype(jnp.bfloat16)
    expert_total = lax.axis_size("sp") * lax.axis_size("tp")
    top_count = route_ids.shape[1]
    capacity = 2 * tok_rows * top_count // expert_total
    flat_ids = route_ids.reshape(-1)
    one_hot = (flat_ids[:, None] == jnp.arange(expert_total, dtype=jnp.int32)[None, :]).astype(
        jnp.int32
    )
    rank = jnp.sum((jnp.cumsum(one_hot, axis=0) - 1) * one_hot, axis=1)
    slot = flat_ids * capacity + rank
    slot_count = expert_total * capacity
    source_row = (
        jnp.zeros((slot_count,), jnp.int32)
        .at[slot]
        .set(jnp.arange(flat_ids.shape[0], dtype=jnp.int32) // top_count)
    )
    filled = jnp.zeros((slot_count,), jnp.bool_).at[slot].set(True)
    outgoing = jnp.where(filled[:, None], normed[source_row], jnp.zeros((), jnp.bfloat16)).reshape(
        expert_total, capacity, width
    )
    arrived = lax.all_to_all(outgoing, ("sp", "tp"), split_axis=0, concat_axis=0, tiled=True)
    sources, items, features = arrived.shape
    rows_in = arrived.reshape(sources * items, features)
    hidden = (
        jax.nn.silu(jnp.dot(rows_in, w_gate[0], preferred_element_type=jnp.float32))
        * jnp.dot(rows_in, w_up[0], preferred_element_type=jnp.float32)
    ).astype(jnp.bfloat16)
    outputs = jnp.dot(hidden, w_down[0], preferred_element_type=jnp.float32).astype(jnp.bfloat16)
    returned = lax.all_to_all(
        outputs.reshape(sources, items, features),
        ("sp", "tp"),
        split_axis=0,
        concat_axis=0,
        tiled=True,
    )
    picked = (
        returned.reshape(slot_count, width)[slot]
        .astype(jnp.float32)
        .reshape(tok_rows, top_count, width)
    )
    expo = jnp.exp(route_logits)
    gate = group_weight[:, None] * expo / jnp.sum(expo, axis=1, keepdims=True)
    result = resid + jnp.sum(gate[:, :, None] * picked, axis=1)
    return result.astype(jnp.bfloat16)


def solution(mesh):
    placed = (
        P(("sp", "tp"), None),
        P("sp", "tp"),
        P("sp", "tp"),
        P("sp", "tp"),
        P("sp"),
        P(None, "tp"),
        P(),
        P(),
        P(("sp", "tp"), None),
        P(("sp", "tp"), None),
        P(("sp", "tp")),
        P(("sp", "tp"), None, None),
        P(("sp", "tp"), None, None),
        P(("sp", "tp"), None, None),
    )
    return jax.shard_map(
        on_device, mesh=mesh, in_specs=placed, out_specs=P(("sp", "tp"), None), check_vma=False
    )
```

profile of v0, /device:TPU:1, one launch (start us, length us, event | category | flops | bytes accessed | tf_op | source)
XLA Modules:
  0.0 151.8 jit_solution(14696057404416062906)
XLA Ops:
  0.0 0.8 convert_element_type.66
  0.8 0.6 fusion.24
  1.4 4.4 %collective-permute-start.1 = (bf16[1]{0:T(256)(128)(2,1)}, bf16[1]{0:T(256)(128)(2,1)}, u32[]{:S(2)}, u32[]{:S(2)}) collective-permute-start(bf16[1]{0:T(256)(128)(2,1)} %get-tuple-element.14), channel_id=1, source_target_pairs={{0,2},{2,4},{4,6},{6,8},{8,10},{10,12},{12,14},{14,16},{16,18},{18... | collective-permute-start | bytes 14 | tf_op jit(solution)/shard_map/ppermute | solution.py:14
  5.8 1.3 collective-permute-start.3
  7.1 1.1 multiply_convert_fusion.3
  8.2 4.0 %collective-permute-start = (bf16[1,512]{1,0:T(2,128)(2,1)S(1)}, bf16[1,512]{1,0:T(2,128)(2,1)S(1)}, u32[]{:S(2)}, u32[]{:S(2)}) collective-permute-start(bf16[1,512]{1,0:T(2,128)(2,1)S(1)} %get-tuple-element.5), channel_id=1, source_target_pairs={{0,2},{2,4},{4,6},{6,8},{8,10},{10,12},{12,14},{14,16},{16,18},{18... | collective-permute-start | bytes 3080 | tf_op jit(solution)/shard_map/ppermute | solution.py:14
  12.2 1.3 collective-permute-start.2
  13.5 0.8 copy.25
  14.3 0.1 eq.37
  14.4 0.1 eq.33
  14.6 0.7 broadcast_multiply_fusion
  15.2 0.8 fusion.23
  16.1 0.1 copy.27
  16.2 0.2 fusion.13
  16.4 0.1 add_add_fusion
  16.5 0.1 copy.24
  16.6 0.1 mul.133
  16.8 0.2 fusion.14
  17.0 1.4 scatter_custom_fusion.1
  18.4 1.5 scatter_custom_fusion
  19.9 0.1 broadcast_in_dim.22
  20.0 0.0 collective-permute-done.1
  20.0 0.0 collective-permute-done.3
  20.1 1.3 pad_maximum_fusion.2
  21.3 0.1 compare_convert_fusion.3
  21.4 0.0 collective-permute-done
  21.4 0.3 multiply_convert_fusion.2
  21.7 5.1 %all_to_all.29 = bf16[2,128,512]{2,1,0:T(8,128)(2,1)S(1)} all-to-all(bf16[2,128,512]{2,1,0:T(8,128)(2,1)S(1)} %bitcast.35), channel_id=1, replica_groups=mesh['sp'=64,'tp'=2] {'tp'}, dimensions={0} | all-to-all | bytes 524288 | tf_op jit(solution)/shard_map/all_to_all | solution.py:51
  26.8 0.2 copy.22
  27.0 0.0 copy-start.3
  27.0 3.0 %multiply_reduce_fusion.1 = (f32[128]{0:T(128)S(1)}, f32[128,2048]{1,0:T(8,128)S(1)}) fusion(bf16[128,1024]{0,1:T(8,128)(2,1)S(1)} %bitcast.36, bf16[1024,2048]{1,0:T(8,128)(2,1)} %param.20, bf16[128,2048]{1,0:T(8,128)(2,1)S(1)} %copy-done.1), kind=kOutput, calls=%fused_computation.17 | convolution fusion | flops 537919360 | bytes 6029824 | tf_op jit(solution)/shard_map/dot_general | solution.py:52
  30.0 0.2 multiply_convert_fusion.1
  30.2 3.3 %gather_fusion = bf16[512,2048]{1,0:T(8,128)(2,1)} fusion(bf16[128,2048]{1,0:T(8,128)(2,1)S(1)} %multiply_convert_fusion.1, s32[1024]{0:T(1024)S(1)} %pad_clamp_fusion.1), kind=kCustom, calls=%fused_computation | custom fusion | bytes 4196352 | tf_op jit(solution)/shard_map/gather | solution.py:72
  33.5 2.7 %gather.9 = bf16[128,4,2048]{2,1,0:T(4,128)(2,1)S(1)} reshape(bf16[512,2048]{1,0:T(8,128)(2,1)} %gather_fusion) | data formatting | bytes 4194304 | tf_op jit(solution)/shard_map/gather | solution.py:72
  36.3 1.0 broadcast_select_fusion
  37.3 44.6 %all_to_all.30 = bf16[128,4,2048]{2,1,0:T(4,128)(2,1)S(1)} all-to-all(bf16[128,4,2048]{2,1,0:T(4,128)(2,1)S(1)} %broadcast_select_fusion), channel_id=1, replica_groups=mesh['sp'=64,'tp'=2] {'sp','tp'}, dimensions={0} | all-to-all | bytes 4194304 | tf_op jit(solution)/shard_map/all_to_all | solution.py:75
  81.9 2.0 %reshape.87 = bf16[512,2048]{1,0:T(8,128)(2,1)} reshape(bf16[128,4,2048]{2,1,0:T(4,128)(2,1)S(1)} %all_to_all.30) | data formatting | bytes 4194304 | tf_op jit(solution)/shard_map/reshape | solution.py:77
  83.9 6.6 %fusion.4 = f32[512,1024]{1,0:T(8,128)} fusion(bf16[512,2048]{1,0:T(8,128)(2,1)} %reshape.87, bf16[1,2048,1024]{2,1,0:T(8,128)(2,1)} %param.25), kind=kOutput, calls=%fused_computation.8 | convolution fusion | flops 2147483648 | bytes 8388608 | tf_op jit(solution)/shard_map/dot_general | solution.py:79
  90.6 9.9 %fusion.6 = bf16[512,2048]{1,0:T(8,128)(2,1)} fusion(bf16[1,1024,2048]{2,1,0:T(8,128)(2,1)} %param.27, f32[512,1024]{1,0:T(8,128)} %fusion.4, bf16[512,2048]{1,0:T(8,128)(2,1)S(1)} %copy-done, bf16[1,2048,1024]{2,1,0:T(8,128)(2,1)} %param.26), kind=kOutput, calls=%fused_computation.10 | convolution fusion | flops 4299161600 | bytes 14680064 | tf_op jit(solution)/shard_map/dot_general | solution.py:82
  100.5 4.1 %reshape.88 = bf16[128,4,2048]{2,1,0:T(4,128)(2,1)} reshape(bf16[512,2048]{1,0:T(8,128)(2,1)} %fusion.6) | data formatting | bytes 4194304 | tf_op jit(solution)/shard_map/reshape | solution.py:84
  104.6 5.6 %all-to-all-start.2 = ((bf16[128,4,2048]{2,1,0:T(4,128)(2,1)}), bf16[128,4,2048]{2,1,0:T(4,128)(2,1)}, u32[]{:S(2)}, u32[]{:S(2)}) async-start(bf16[128,4,2048]{2,1,0:T(4,128)(2,1)} %reshape.88), calls=%async_computation.2 | async-start | bytes 4194304 | tf_op jit(solution)/shard_map/all_to_all | solution.py:83
  110.3 0.1 copy.23
  110.4 30.1 %all-to-all-done.2 = bf16[128,4,2048]{2,1,0:T(4,128)(2,1)} async-done(((bf16[128,4,2048]{2,1,0:T(4,128)(2,1)}), bf16[128,4,2048]{2,1,0:T(4,128)(2,1)}, u32[]{:S(2)}, u32[]{:S(2)}) %all-to-all-start.2) | async-done | bytes 2097184 | tf_op jit(solution)/shard_map/all_to_all | solution.py:83
  140.5 2.5 %reshape.89 = bf16[512,2048]{1,0:T(8,128)(2,1)S(1)} reshape(bf16[128,4,2048]{2,1,0:T(4,128)(2,1)} %all-to-all-done.2) | data formatting | bytes 4194304 | tf_op jit(solution)/shard_map/reshape | solution.py:91
  143.0 2.3 %gather_fusion.1 = bf16[256,2048]{1,0:T(8,128)(2,1)} fusion(bf16[512,2048]{1,0:T(8,128)(2,1)S(1)} %reshape.89, s32[1024]{0:T(1024)S(1)} %pad_clamp_fusion), kind=kCustom, calls=%fused_computation.1 | custom fusion | bytes 2098176 | tf_op jit(solution)/shard_map/gather | solution.py:91
  145.4 2.4 %reshape.90 = f32[128,2,2048]{2,1,0:T(2,128)S(1)} reshape(bf16[256,2048]{1,0:T(8,128)(2,1)} %gather_fusion.1) | data formatting | bytes 3145728 | tf_op jit(solution)/shard_map/convert_element_type | solution.py:92
  147.7 3.2 %multiply_reduce_fusion = f32[128,2048]{1,0:T(8,128)S(1)} fusion(f32[128,2,2048]{2,1,0:T(2,128)S(1)} %reshape.90, f32[128,2]{1,0:T(8,128)S(1)} %copy.23), kind=kLoop, calls=%fused_computation.12 | loop fusion | flops 786432 | bytes 3146752 | tf_op jit(solution)/shard_map/reduce_sum | solution.py:97
  150.9 0.9 add_convert_fusion
  (28 shorter events, 0.2 us)
Async XLA Ops:
  0.0 21.3 %copy-start.5 = (s32[256]{0:T(256)S(1)}, s32[256]{0:T(256)}, u32[]{:S(2)}) copy-start(s32[256]{0:T(256)} %param.18) | copy-start | bytes 3076
  0.0 21.4 %copy-start.2 = (bf16[256,512]{1,0:T(8,128)(2,1)S(1)}, bf16[256,512]{1,0:T(8,128)(2,1)}, u32[]{:S(2)}) copy-start(bf16[256,512]{1,0:T(8,128)(2,1)} %param.15) | copy-start | bytes 786436
  0.0 27.0 %copy-start.1 = (bf16[128,2048]{1,0:T(8,128)(2,1)S(1)}, bf16[128,2048]{1,0:T(8,128)(2,1)}, u32[]{:S(2)}) copy-start(bf16[128,2048]{1,0:T(8,128)(2,1)} %param.14) | copy-start | bytes 1572868
  1.4 18.7 %collective-permute-start.1 = (bf16[1]{0:T(256)(128)(2,1)}, bf16[1]{0:T(256)(128)(2,1)}, u32[]{:S(2)}, u32[]{:S(2)}) collective-permute-start(bf16[1]{0:T(256)(128)(2,1)} %get-tuple-element.14), channel_id=1, source_target_pairs={{0,2},{2,4},{4,6},{6,8},{8,10},{10,12},{12,14},{14,16},{16,18},{18... | collective-permute-start | bytes 14 | tf_op jit(solution)/shard_map/ppermute | solution.py:14
  5.8 14.3 %collective-permute-start.3 = (bf16[1]{0:T(256)(128)(2,1)}, bf16[1]{0:T(256)(128)(2,1)}, u32[]{:S(2)}, u32[]{:S(2)}) collective-permute-start(bf16[1]{0:T(256)(128)(2,1)} %get-tuple-element.15), channel_id=1, source_target_pairs={{2,0},{4,2},{6,4},{8,6},{10,8},{12,10},{14,12},{16,14},{18,16},{20... | collective-permute-start | bytes 14 | tf_op jit(solution)/shard_map/ppermute | solution.py:15
  8.2 13.2 %collective-permute-start = (bf16[1,512]{1,0:T(2,128)(2,1)S(1)}, bf16[1,512]{1,0:T(2,128)(2,1)S(1)}, u32[]{:S(2)}, u32[]{:S(2)}) collective-permute-start(bf16[1,512]{1,0:T(2,128)(2,1)S(1)} %get-tuple-element.5), channel_id=1, source_target_pairs={{0,2},{2,4},{4,6},{6,8},{8,10},{10,12},{12,14},{14,16},{16,18},{18... | collective-permute-start | bytes 3080 | tf_op jit(solution)/shard_map/ppermute | solution.py:14
  12.2 9.2 %collective-permute-start.2 = (bf16[1,512]{1,0:T(2,128)(2,1)S(1)}, bf16[1,512]{1,0:T(2,128)(2,1)S(1)}, u32[]{:S(2)}, u32[]{:S(2)}) collective-permute-start(bf16[1,512]{1,0:T(2,128)(2,1)S(1)} %get-tuple-element.6), channel_id=1, source_target_pairs={{2,0},{4,2},{6,4},{8,6},{10,8},{12,10},{14,12},{16,14},{18,16},{20... | collective-permute-start | bytes 3080 | tf_op jit(solution)/shard_map/ppermute | solution.py:15
  27.0 3.0 %copy-start.3 = (f32[2048]{0:T(1024)S(1)}, f32[2048]{0:T(1024)}, u32[]{:S(2)}) copy-start(f32[2048]{0:T(1024)} %param.21) | copy-start | bytes 24580
  83.9 6.7 %copy-start = (bf16[512,2048]{1,0:T(8,128)(2,1)S(1)}, bf16[512,2048]{1,0:T(8,128)(2,1)}, u32[]{:S(2)}) copy-start(bf16[512,2048]{1,0:T(8,128)(2,1)} %reshape.87) | copy-start | bytes 6291460
  104.6 5.6 %copy-start.4 = (f32[128,2]{0,1:T(2,128)S(1)}, f32[128,2]{0,1:T(2,128)}, u32[]{:S(2)}) copy-start(f32[128,2]{0,1:T(2,128)} %param.23) | copy-start | bytes 3076
  104.6 5.6 %copy-start.6 = (f32[128]{0:T(128)S(1)}, f32[128]{0:T(128)}, u32[]{:S(2)}) copy-start(f32[128]{0:T(128)} %param.24) | copy-start | bytes 1540
  104.6 35.9 %all-to-all-start.2 = ((bf16[128,4,2048]{2,1,0:T(4,128)(2,1)}), bf16[128,4,2048]{2,1,0:T(4,128)(2,1)}, u32[]{:S(2)}, u32[]{:S(2)}) async-start(bf16[128,4,2048]{2,1,0:T(4,128)(2,1)} %reshape.88), calls=%async_computation.2 | async-start | bytes 4194304 | tf_op jit(solution)/shard_map/all_to_all | solution.py:83
where the time goes:
time: 152 us
  blocking collectives  49.7 us (33%)
  waiting for transfers between devices  30.1 us (20%)
  local copies, waits for them, and re-layouts  25.7 us (17%)
  matrix products  19.6 us (13%)
  starting transfers between devices  16.6 us (11%)
  other arithmetic  9.95 us (7%)
    all_to_all x1, blocking collectives, on_device(): lax.all_to_all(outgoing, ('sp', 'tp'), split_axis=0, concat_axis=0, tiled...  44.6 us
    all_to_all x1, waiting for transfers between devices, on_device(): lax.all_to_all(outputs.reshape(sources, items, features), ('sp', 'tp'), s...  30.1 us
    dot_general x1, matrix products, on_device(): jnp.dot(hidden, w_down[0], preferred_element_type=jnp.float32)  9.9 us
    ppermute x2, starting transfers between devices, padded_2(): before = lax.ppermute(last, axis, up)  8.41 us
    dot_general x1, matrix products, on_device(): jnp.dot(rows_in, w_gate[0], preferred_element_type=jnp.float32)  6.65 us
    gather x2, local copies, waits for them, and re-layouts, on_device(): normed[source_row]  6.08 us
    all_to_all x1, starting transfers between devices, on_device(): lax.all_to_all(outputs.reshape(sources, items, features), ('sp', 'tp'), s...  5.6 us
    all_to_all x1, blocking collectives, on_device(): lax.all_to_all(mixed, 'tp', split_axis=0, concat_axis=1, tiled=True)  5.1 us
  transfers between devices with their start and end apart: 5, of which 1 were waited for; matrix products, arithmetic and copies ran while one was open for 6% of the time, Pallas kernels for 0%

commit v1 on v0

v1 whole, which is shorter than its diff:
```python
import functools

import jax
import jax.numpy as jnp
from jax import lax
from jax.experimental import pallas as pl
from jax.experimental.pallas import tpu as pltpu
from jax.sharding import PartitionSpec as P

MESH = pl.DeviceIdType.MESH
STEP = 37
BACK = pow(STEP, -1, 128)
CHUNKS = 4
PER = 32
F32 = jnp.float32
BF = jnp.bfloat16


def padded_2(shard, sides, width):
    for axis, dim in sides:
        size, length = (lax.axis_size(axis), shard.shape[dim])
        up = [(i, (i + 1) % size) for i in range(size - 1)]
        down = [(j, i) for i, j in up]
        last = lax.slice_in_dim(shard, length - width, length, axis=dim)
        leading = lax.slice_in_dim(shard, 0, width, axis=dim)
        before = lax.ppermute(last, axis, up)
        after = lax.ppermute(leading, axis, down)
        shard = jnp.concatenate([before, shard, after], axis=dim)
    return shard


def partner(k, sign, sp, tp):
    o = lax.rem(k * STEP, 128)
    dz, dy, dx, dc = o // 32, lax.rem(o // 8, 4), lax.rem(o // 2, 4), lax.rem(o, 2)
    z, y, x = sp // 16, lax.rem(sp // 4, 4), lax.rem(sp, 4)
    if sign < 0:
        dz, dy, dx = 4 - dz, 4 - dy, 4 - dx
    there = lax.rem(z + dz, 4) * 16 + lax.rem(y + dy, 4) * 4 + lax.rem(x + dx, 4)
    return there, lax.rem(tp + dc, 2)


def dot(a, b):
    return jnp.dot(a, b, preferred_element_type=F32)


def iota(shape, dim):
    return lax.broadcasted_iota(jnp.int32, shape, dim)


def to_row(col, eye):
    return jnp.sum(jnp.where(eye, col, 0.0), axis=0, keepdims=True)


def to_col(row, eye):
    return jnp.sum(jnp.where(eye, row, 0.0), axis=1, keepdims=True)


def kernel(
    normed_ref, resid_ref, ids_ref, logits_ref, gw_ref, wg_hbm, wu_hbm, wd_hbm,
    out_ref,
    wg, wu, wd, nq, fold, unfold, outbox, inbox, outbox2, inbox2, xbuf, hbuf, yq, acc,
    wsem, send1, recv1, send2, recv2,
):
    sp, tp = lax.axis_index("sp"), lax.axis_index("tp")
    loads = [
        pltpu.make_async_copy(wg_hbm.at[0], wg, wsem.at[0]),
        pltpu.make_async_copy(wu_hbm.at[0], wu, wsem.at[1]),
        pltpu.make_async_copy(wd_hbm.at[0], wd, wsem.at[2]),
    ]
    for load in loads:
        load.start()
    barrier = pltpu.get_barrier_semaphore()

    @pl.loop(1, 128)
    def _(k):
        pl.semaphore_signal(barrier, inc=1, device_id=partner(k, 1, sp, tp), device_id_type=MESH)

    eye = iota((128, 128), 0) == iota((128, 128), 1)
    lane = iota((128, 128), 1)
    hot = [(ids_ref[:, k:k + 1] == lane).astype(F32) for k in range(2)]
    before = (iota((128, 128), 0) > lane).astype(BF)
    count = dot(before, (hot[0] + hot[1]).astype(BF))
    z, y, x = sp // 16, lax.rem(sp // 4, 4), lax.rem(sp, 4)
    slots, slot_rows = [], []
    for k in range(2):
        e = ids_ref[:, k:k + 1]
        dz = ((e >> 5) + (4 - z)) & 3
        dy = (((e >> 3) & 3) + (4 - y)) & 3
        dx = (((e >> 1) & 3) + (4 - x)) & 3
        dc = ((e & 1) + (2 - tp)) & 1
        o = dz * 32 + dy * 8 + dx * 2 + dc
        place = (o * BACK) & 127
        rank = jnp.sum(hot[k] * count, axis=1, keepdims=True)
        slot = place.astype(F32) * 4.0 + rank
        slots.append(slot.astype(jnp.int32))
        slot_rows.append(to_row(slot, eye).astype(jnp.int32))
    expo = jnp.exp(logits_ref[...])
    gw = to_col(gw_ref[...], eye)
    total = expo[:, 0:1] + expo[:, 1:2]
    gates = [gw * expo[:, k:k + 1] / total for k in range(2)]

    for q in range(4):
        nq[q * 128:(q + 1) * 128, :] = normed_ref[:, q * 512:(q + 1) * 512]
    m = iota((512, 512), 0)
    n = iota((512, 512), 1)
    fold[...] = (m == (n & 127) * 4 + (n >> 7)).astype(BF)
    unfold[...] = (n == (m & 127) * 4 + (m >> 7)).astype(BF)

    def copy_out(k, c):
        rows = pl.ds(pl.multiple_of(k * 16, 16), 16)
        return pltpu.make_async_remote_copy(
            src_ref=outbox.at[rows], dst_ref=inbox.at[rows], send_sem=send1.at[c], recv_sem=recv1.at[c],
            device_id=partner(k, 1, sp, tp), device_id_type=MESH)

    def copy_back(k, c):
        rows = pl.ds(pl.multiple_of(k * 16, 16), 16)
        return pltpu.make_async_remote_copy(
            src_ref=outbox2.at[rows], dst_ref=inbox2.at[rows], send_sem=send2.at[c], recv_sem=recv2.at[c],
            device_id=partner(k, -1, sp, tp), device_id_type=MESH)

    def pack(c):
        base = c * 512
        at = iota((512, 128), 0) + base
        mine = ((at >> 2) == slot_rows[0]) | ((at >> 2) == slot_rows[1])
        picks = [(mine & ((at & 3) == q)).astype(BF) for q in range(4)]
        packed = dot(jnp.concatenate(picks, axis=1), nq[...])
        outbox[base:base + 512, :] = packed.astype(BF)

    def span(c):
        return pl.ds(16 if c == 0 else c * 512, 496 if c == 0 else 512)

    pack(0)
    pl.semaphore_wait(barrier, 127)
    for c in range(CHUNKS):
        @pl.loop(max(1, c * PER), (c + 1) * PER)
        def _(k):
            copy_out(k, c).start()
        if c + 1 < CHUNKS:
            pack(c + 1)
    inbox[0:16, :] = outbox[0:16, :]
    for load in loads:
        load.wait()

    for c in range(CHUNKS):
        s = span(c)
        pltpu.make_async_copy(inbox.at[s], inbox.at[s], recv1.at[c]).wait()
        for q in range(4):
            xq = dot(unfold[q * 128:(q + 1) * 128, :], inbox[c * 512:(c + 1) * 512, :])
            xbuf[:, q * 512:(q + 1) * 512] = xq.astype(BF)

        @pl.loop(0, 4)
        def _(n):
            cols = pl.ds(pl.multiple_of(n * 256, 256), 256)
            g = dot(xbuf[...], wg[:, cols])
            u = dot(xbuf[...], wu[:, cols])
            hbuf[:, cols] = (g / (1.0 + jnp.exp(-g)) * u).astype(BF)

        @pl.loop(0, 4)
        def _(q):
            cols = pl.ds(pl.multiple_of(q * 512, 512), 512)
            rows = pl.ds(pl.multiple_of(q * 128, 128), 128)
            yq[rows, :] = dot(hbuf[...], wd[:, cols]).astype(BF)

        outbox2[c * 512:(c + 1) * 512, :] = dot(fold[...], yq[...]).astype(BF)

        @pl.loop(max(1, c * PER), (c + 1) * PER)
        def _(k):
            copy_back(k, c).start()
    inbox2[0:16, :] = outbox2[0:16, :]

    for c in range(CHUNKS):
        s = span(c)
        pltpu.make_async_copy(inbox2.at[s], inbox2.at[s], recv2.at[c]).wait()
        at = iota((128, 512), 1) + c * 512
        for q in range(4):
            cols = slice(q * 512, (q + 1) * 512)
            pick = jnp.concatenate([(at == slots[k] * 4 + q).astype(BF) for k in range(2)], axis=0)
            found = dot(pick, inbox2[c * 512:(c + 1) * 512, :])
            if c == 0:
                acc[:, cols] = found
            elif c + 1 < CHUNKS:
                acc[:, cols] += found
            else:
                found = found + acc[:, cols]
                out_ref[:, cols] = (
                    resid_ref[:, cols] + (gates[0] * found[:128] + gates[1] * found[128:])).astype(BF)
    for c in range(CHUNKS):
        s = span(c)
        pltpu.make_async_copy(outbox.at[s], outbox.at[s], send1.at[c]).wait()
        pltpu.make_async_copy(outbox2.at[s], outbox2.at[s], send2.at[c]).wait()


def experts(normed, resid, ids, logits, gw, w_gate, w_up, w_down):
    vmem = pl.BlockSpec(memory_space=pltpu.VMEM)
    hbm = pl.BlockSpec(memory_space=pl.ANY)
    box = pltpu.VMEM((2048, 512), BF)
    sems = pltpu.SemaphoreType.DMA((CHUNKS,))
    return pl.pallas_call(
        kernel,
        out_shape=jax.ShapeDtypeStruct((128, 2048), BF),
        in_specs=[vmem] * 5 + [hbm] * 3,
        out_specs=vmem,
        scratch_shapes=[
            pltpu.VMEM((2048, 1024), BF), pltpu.VMEM((2048, 1024), BF), pltpu.VMEM((1024, 2048), BF),
            pltpu.VMEM((512, 512), BF), pltpu.VMEM((512, 512), BF), pltpu.VMEM((512, 512), BF),
            box, box, box, box,
            pltpu.VMEM((128, 2048), BF), pltpu.VMEM((128, 1024), BF), pltpu.VMEM((512, 512), BF),
            pltpu.VMEM((256, 2048), F32),
            pltpu.SemaphoreType.DMA((3,)), sems, sems, sems, sems,
        ],
        compiler_params=pltpu.CompilerParams(
            collective_id=0, has_side_effects=True, vmem_limit_bytes=50 * 2**20),
        name="experts",
    )(normed, resid, ids, logits, gw, w_gate, w_up, w_down)


def on_device(
    stream, outer_gate, inner_gate, conv_values, doc_ids, conv_taps, out_weight, norm_gain,
    route_ids, route_logits, group_weight, w_gate, w_up, w_down,
):
    product = (inner_gate.astype(F32) * conv_values.astype(F32)).astype(BF)
    doc_float = doc_ids.astype(BF)
    padded, padded_docs = (padded_2(product, (("sp", 0),), 1), padded_2(doc_float, (("sp", 0),), 1))
    same_prev = (padded_docs[:-2] == doc_float).astype(F32)[:, None]
    same_next = (padded_docs[2:] == doc_float).astype(F32)[:, None]
    conv = (
        conv_taps[0] * padded[:-2].astype(F32) * same_prev
        + conv_taps[1] * product.astype(F32)
        + conv_taps[2] * padded[2:].astype(F32) * same_next
    )
    mixed = (outer_gate.astype(F32) * conv).astype(BF)
    channels = lax.all_to_all(mixed, "tp", split_axis=0, concat_axis=1, tiled=True)
    projected = jnp.dot(channels, out_weight, preferred_element_type=F32)
    resid = stream.astype(F32) + projected
    scale = lax.rsqrt(jnp.mean(resid * resid, axis=-1, keepdims=True) + 1e-06)
    normed = (resid * scale * norm_gain).astype(BF)
    return experts(
        normed, resid, route_ids, route_logits, group_weight.reshape(1, 128), w_gate, w_up, w_down)


def solution(mesh):
    placed = (
        P(("sp", "tp"), None),
        P("sp", "tp"),
        P("sp", "tp"),
        P("sp", "tp"),
        P("sp"),
        P(None, "tp"),
        P(),
        P(),
        P(("sp", "tp"), None),
        P(("sp", "tp"), None),
        P(("sp", "tp")),
        P(("sp", "tp"), None, None),
        P(("sp", "tp"), None, None),
        P(("sp", "tp"), None, None),
    )
    return jax.shard_map(
        on_device, mesh=mesh, in_specs=placed, out_specs=P(("sp", "tp"), None), check_vma=False
    )
```

time: 152 us -> 103 us (0.68)
  the two profiles are of different devices: /device:TPU:1 before, /device:TPU:19 now
where the time goes in v1:
time: 103 us; the launch traced here: 102 us
  Pallas kernels  73.4 us (71%)
  starting transfers between devices  11.5 us (11%)
  other arithmetic  5.25 us (5%)
  blocking collectives  5.1 us (5%)
  local copies, waits for them, and re-layouts  3.96 us (4%)
  matrix products  3.13 us (3%)
    pallas_call x1, Pallas kernels, experts(): pl.pallas_call(kernel, out_shape=jax.ShapeDtypeStruct((128, 2048), BF), i...  73.4 us
    ppermute x2, starting transfers between devices, padded_2(): before = lax.ppermute(last, axis, up)  6.23 us
    ppermute x2, starting transfers between devices, padded_2(): after = lax.ppermute(leading, axis, down)  5.24 us
    all_to_all x1, blocking collectives, on_device(): lax.all_to_all(mixed, 'tp', split_axis=0, concat_axis=1, tiled=True)  5.1 us
    dot_general x1, matrix products, on_device(): projected = jnp.dot(channels, out_weight, preferred_element_type=F32)  3.13 us
    unnamed x7, local copies, waits for them, and re-layouts  2.37 us
  transfers between devices with their start and end apart: 4, of which 0 were waited for; matrix products, arithmetic and copies ran while one was open for 5% of the time, Pallas kernels for 0%

profile of v1, /device:TPU:19, one launch (start us, length us, event | category | flops | bytes accessed | tf_op | source)
XLA Modules:
  0.0 102.4 jit_solution(9060784533544725070)
XLA Ops:
  0.0 0.7 convert_element_type.45
  0.7 0.6 fusion.2
  1.3 3.1 %collective-permute-start.1 = (bf16[1]{0:T(256)(128)(2,1)}, bf16[1]{0:T(256)(128)(2,1)}, u32[]{:S(2)}, u32[]{:S(2)}) collective-permute-start(bf16[1]{0:T(256)(128)(2,1)} %get-tuple-element.14), channel_id=1, source_target_pairs={{0,2},{2,4},{4,6},{6,8},{8,10},{10,12},{12,14},{14,16},{16,18},{18... | collective-permute-start | bytes 14 | tf_op jit(solution)/shard_map/ppermute | solution.py:26
  4.4 2.2 %collective-permute-start.3 = (bf16[1]{0:T(256)(128)(2,1)}, bf16[1]{0:T(256)(128)(2,1)}, u32[]{:S(2)}, u32[]{:S(2)}) collective-permute-start(bf16[1]{0:T(256)(128)(2,1)} %get-tuple-element.15), channel_id=1, source_target_pairs={{2,0},{4,2},{6,4},{8,6},{10,8},{12,10},{14,12},{16,14},{18,16},{20... | collective-permute-start | bytes 14 | tf_op jit(solution)/shard_map/ppermute | solution.py:27
  6.6 1.1 %multiply_convert_fusion.2 = bf16[256,512]{1,0:T(8,128)(2,1)S(1)} fusion(bf16[256,512]{1,0:T(8,128)(2,1)} %param.17, bf16[256,512]{1,0:T(8,128)(2,1)} %param.16), kind=kLoop, calls=%fused_computation.4 | loop fusion | flops 524288 | bytes 786432 | tf_op jit(solution)/shard_map/convert_element_type | solution.py:221
  7.7 0.0 copy-start.1
  7.7 3.1 %collective-permute-start = (bf16[1,512]{1,0:T(2,128)(2,1)S(1)}, bf16[1,512]{1,0:T(2,128)(2,1)S(1)}, u32[]{:S(2)}, u32[]{:S(2)}) collective-permute-start(bf16[1,512]{1,0:T(2,128)(2,1)S(1)} %get-tuple-element.5), channel_id=1, source_target_pairs={{0,2},{2,4},{4,6},{6,8},{8,10},{10,12},{12,14},{14,16},{16,18},{18... | collective-permute-start | bytes 3080 | tf_op jit(solution)/shard_map/ppermute | solution.py:26
  10.8 3.1 %collective-permute-start.2 = (bf16[1,512]{1,0:T(2,128)(2,1)S(1)}, bf16[1,512]{1,0:T(2,128)(2,1)S(1)}, u32[]{:S(2)}, u32[]{:S(2)}) collective-permute-start(bf16[1,512]{1,0:T(2,128)(2,1)S(1)} %get-tuple-element.6), channel_id=1, source_target_pairs={{2,0},{4,2},{6,4},{8,6},{10,8},{12,10},{14,12},{16,14},{18,16},{20... | collective-permute-start | bytes 3080 | tf_op jit(solution)/shard_map/ppermute | solution.py:27
  13.9 0.8 fusion.1
  14.7 0.8 copy.20.ids_ref
  15.5 0.8 copy.21.logits_ref
  16.3 0.0 collective-permute-done.1
  16.3 0.0 collective-permute-done.3
  16.3 1.3 %pad_maximum_fusion.2 = (bf16[257]{0:T(512)(128)(2,1)S(1)}, bf16[257]{0:T(512)(128)(2,1)S(1)}) fusion(bf16[256]{0:T(256)(128)(2,1)S(1)} %convert_element_type.45, bf16[1]{0:T(256)(128)(2,1)} %collective-permute-done.1, bf16[1]{0:T(256)(128)(2,1)} %collective-permute-done.3), kind=kLoop, calls=%fused_computation.9 | loop fusion | flops 2056 | bytes 1544 | tf_op jit(solution)/shard_map/concatenate | solution.py:28
  17.6 0.8 compare_convert_fusion.1
  18.4 0.0 collective-permute-done
  18.4 0.0 collective-permute-done.2
  18.4 1.2 %multiply_convert_fusion.1 = bf16[256,512]{1,0:T(8,128)(2,1)S(1)} fusion(bf16[256,512]{1,0:T(8,128)(2,1)S(1)} %multiply_convert_fusion.2, bf16[256,512]{1,0:T(8,128)(2,1)} %param.15, bf16[1,512]{1,0:T(2,128)(2,1)S(1)} %collective-permute-done.2, bf16[1,512]{1,0:T(2,128)(2,1)S(1)} %collective-permute-done, f32[256]{0:T(256)S(1)} %get-tuple-element.11, ...), kind=kLoop, calls=%fused_computation.3 | loop fusion | flops 2490368 | bytes 796672 | tf_op jit(solution)/shard_map/convert_element_type | solution.py:231
  19.6 5.1 %all_to_all.19 = bf16[2,128,512]{2,1,0:T(8,128)(2,1)S(1)} all-to-all(bf16[2,128,512]{2,1,0:T(8,128)(2,1)S(1)} %bitcast.10), channel_id=1, replica_groups=mesh['sp'=64,'tp'=2] {'tp'}, dimensions={0} | all-to-all | bytes 524288 | tf_op jit(solution)/shard_map/all_to_all | solution.py:232
  24.7 0.0 copy-start
  24.7 0.2 copy.19
  24.9 3.1 %multiply_reduce_fusion = (f32[128]{0:T(128)S(1)}, f32[128,2048]{1,0:T(8,128)S(1)}) fusion(bf16[128,1024]{0,1:T(8,128)(2,1)S(1)} %bitcast.11, bf16[1024,2048]{1,0:T(8,128)(2,1)} %param.20, bf16[128,2048]{1,0:T(8,128)(2,1)} %param.14), kind=kOutput, calls=%fused_computation.2 | convolution fusion | flops 537919360 | bytes 6029824 | tf_op jit(solution)/shard_map/dot_general | solution.py:233
  28.0 0.0 copy-done.1
  28.1 0.2 multiply_convert_fusion.normed_ref
  28.2 0.0 copy-done
  28.2 73.4 %experts.1 = bf16[128,2048]{1,0:T(8,128)(2,1)S(1)} custom-call(bf16[128,2048]{1,0:T(8,128)(2,1)S(1)} %multiply_convert_fusion.normed_ref, f32[128,2048]{1,0:T(8,128)S(1)} %get-tuple-element.17.resid_ref, s32[128,2]{1,0:T(8,128)S(1)} %copy.20.ids_ref, f32[128,2]{1,0:T(8,128)S(1)} %copy.21.logits_ref, f32[1,128]{1,0:T(1,128)S(1)} %bitcast.9, ...), custom_call_target="tpu_custom_call" | custom-call | tf_op jit(solution)/shard_map/experts/pallas_call | solution.py:198
  101.6 0.8 copy.23
  (2 shorter events, 0.0 us)
Async XLA Ops:
  1.3 15.0 %collective-permute-start.1 = (bf16[1]{0:T(256)(128)(2,1)}, bf16[1]{0:T(256)(128)(2,1)}, u32[]{:S(2)}, u32[]{:S(2)}) collective-permute-start(bf16[1]{0:T(256)(128)(2,1)} %get-tuple-element.14), channel_id=1, source_target_pairs={{0,2},{2,4},{4,6},{6,8},{8,10},{10,12},{12,14},{14,16},{16,18},{18... | collective-permute-start | bytes 14 | tf_op jit(solution)/shard_map/ppermute | solution.py:26
  4.4 11.9 %collective-permute-start.3 = (bf16[1]{0:T(256)(128)(2,1)}, bf16[1]{0:T(256)(128)(2,1)}, u32[]{:S(2)}, u32[]{:S(2)}) collective-permute-start(bf16[1]{0:T(256)(128)(2,1)} %get-tuple-element.15), channel_id=1, source_target_pairs={{2,0},{4,2},{6,4},{8,6},{10,8},{12,10},{14,12},{16,14},{18,16},{20... | collective-permute-start | bytes 14 | tf_op jit(solution)/shard_map/ppermute | solution.py:27
  7.7 20.4 %copy-start.1 = (f32[2048]{0:T(1024)S(1)}, f32[2048]{0:T(1024)}, u32[]{:S(2)}) copy-start(f32[2048]{0:T(1024)} %param.21) | copy-start | bytes 24580
  7.7 10.7 %collective-permute-start = (bf16[1,512]{1,0:T(2,128)(2,1)S(1)}, bf16[1,512]{1,0:T(2,128)(2,1)S(1)}, u32[]{:S(2)}, u32[]{:S(2)}) collective-permute-start(bf16[1,512]{1,0:T(2,128)(2,1)S(1)} %get-tuple-element.5), channel_id=1, source_target_pairs={{0,2},{2,4},{4,6},{6,8},{8,10},{10,12},{12,14},{14,16},{16,18},{18... | collective-permute-start | bytes 3080 | tf_op jit(solution)/shard_map/ppermute | solution.py:26
  10.8 7.6 %collective-permute-start.2 = (bf16[1,512]{1,0:T(2,128)(2,1)S(1)}, bf16[1,512]{1,0:T(2,128)(2,1)S(1)}, u32[]{:S(2)}, u32[]{:S(2)}) collective-permute-start(bf16[1,512]{1,0:T(2,128)(2,1)S(1)} %get-tuple-element.6), channel_id=1, source_target_pairs={{2,0},{4,2},{6,4},{8,6},{10,8},{12,10},{14,12},{16,14},{18,16},{20... | collective-permute-start | bytes 3080 | tf_op jit(solution)/shard_map/ppermute | solution.py:27
  24.7 3.5 %copy-start = (f32[128]{0:T(128)S(1)}, f32[128]{0:T(128)}, u32[]{:S(2)}) copy-start(f32[128]{0:T(128)} %param.24) | copy-start | bytes 1540

commit v2 on v1

--- a/solution.py
+++ b/solution.py
@@ -14,19 +14,6 @@
 PER = 32
 F32 = jnp.float32
 BF = jnp.bfloat16
-
-
-def padded_2(shard, sides, width):
-    for axis, dim in sides:
-        size, length = (lax.axis_size(axis), shard.shape[dim])
-        up = [(i, (i + 1) % size) for i in range(size - 1)]
-        down = [(j, i) for i, j in up]
-        last = lax.slice_in_dim(shard, length - width, length, axis=dim)
-        leading = lax.slice_in_dim(shard, 0, width, axis=dim)
-        before = lax.ppermute(last, axis, up)
-        after = lax.ppermute(leading, axis, down)
-        shard = jnp.concatenate([before, shard, after], axis=dim)
-    return shard
 
 
 def partner(k, sign, sp, tp):
@@ -56,17 +43,22 @@
 
 
 def kernel(
-    normed_ref, resid_ref, ids_ref, logits_ref, gw_ref, wg_hbm, wu_hbm, wd_hbm,
+    stream_hbm, outer_hbm, inner_hbm, values_hbm, docs_hbm, taps_hbm, gain_hbm, ids_hbm, logits_hbm, gw_hbm,
+    ow_hbm, wg_hbm, wu_hbm, wd_hbm,
     out_ref,
-    wg, wu, wd, nq, fold, unfold, outbox, inbox, outbox2, inbox2, xbuf, hbuf, yq, acc,
-    wsem, send1, recv1, send2, recv2,
+    inner_ref, values_ref, docs_ref, outer_ref, taps_ref, ids_ref, logits_ref, gw_ref, stream_ref, gain_ref,
+    ow, wg, wu, wd, product, mixed, edge_prev, edge_next, docs_prev, docs_next, theirs, resid,
+    nq, fold, unfold, outbox, inbox, outbox2, inbox2, xbuf, hbuf, yq, acc,
+    wsem, esend, erecv, tsend, trecv, send1, recv1, send2, recv2,
 ):
     sp, tp = lax.axis_index("sp"), lax.axis_index("tp")
-    loads = [
-        pltpu.make_async_copy(wg_hbm.at[0], wg, wsem.at[0]),
-        pltpu.make_async_copy(wu_hbm.at[0], wu, wsem.at[1]),
-        pltpu.make_async_copy(wd_hbm.at[0], wd, wsem.at[2]),
+    pairs = [
+        (inner_hbm, inner_ref), (values_hbm, values_ref), (docs_hbm, docs_ref), (outer_hbm, outer_ref),
+        (taps_hbm, taps_ref), (ids_hbm, ids_ref), (logits_hbm, logits_ref), (gw_hbm, gw_ref),
+        (stream_hbm, stream_ref), (gain_hbm, gain_ref), (ow_hbm, ow),
+        (wg_hbm.at[0], wg), (wu_hbm.at[0], wu), (wd_hbm.at[0], wd),
     ]
+    loads = [pltpu.make_async_copy(a, b, wsem.at[i]) for i, (a, b) in enumerate(pairs)]
     for load in loads:
         load.start()
     barrier = pltpu.get_barrier_semaphore()
@@ -75,15 +67,42 @@
     def _(k):
         pl.semaphore_signal(barrier, inc=1, device_id=partner(k, 1, sp, tp), device_id_type=MESH)
 
+    for load in loads[:5]:
+        load.wait()
+    product[...] = (inner_ref[...].astype(F32) * values_ref[...].astype(F32)).astype(BF)
+    r0, r1 = iota((256, 256), 0), iota((256, 256), 1)
+    docs = docs_ref[...].astype(F32)
+    doc = to_col(docs, r0 == r1)
+    row = iota((256, 1), 0)
+    same_prev = (to_col(docs, r0 == r1 + 1) == doc).astype(F32)
+    same_next = (to_col(docs, r0 + 1 == r1) == doc).astype(F32)
+
+    def mix(lo, size, first, last, before, after):
+        rows = slice(lo, lo + size)
+        own = product[rows, :].astype(F32)
+        up, down = pltpu.roll(own, 1, 0), pltpu.roll(own, size - 1, 0)
+        at = iota((size, 1), 0)
+        if first is not None:
+            up = jnp.where(at == 0, first, up)
+        if last is not None:
+            down = jnp.where(at == size - 1, last, down)
+        conv = taps_ref[0:1, :] * up * before + taps_ref[1:2, :] * own + taps_ref[2:3, :] * down * after
+        return (outer_ref[rows, :].astype(F32) * conv).astype(BF)
+
+    mixed[...] = mix(0, 256, None, None, same_prev, same_next)
+
+    for load in loads[5:8]:
+        load.wait()
     eye = iota((128, 128), 0) == iota((128, 128), 1)
     lane = iota((128, 128), 1)
-    hot = [(ids_ref[:, k:k + 1] == lane).astype(F32) for k in range(2)]
+    ids = [to_col(ids_ref[k:k + 1, :].astype(F32), eye).astype(jnp.int32) for k in range(2)]
+    hot = [(ids[k] == lane).astype(F32) for k in range(2)]
     before = (iota((128, 128), 0) > lane).astype(BF)
     count = dot(before, (hot[0] + hot[1]).astype(BF))
     z, y, x = sp // 16, lax.rem(sp // 4, 4), lax.rem(sp, 4)
     slots, slot_rows = [], []
     for k in range(2):
-        e = ids_ref[:, k:k + 1]
+        e = ids[k]
         dz = ((e >> 5) + (4 - z)) & 3
         dy = (((e >> 3) & 3) + (4 - y)) & 3
         dx = (((e >> 1) & 3) + (4 - x)) & 3
@@ -95,12 +114,8 @@
         slots.append(slot.astype(jnp.int32))
         slot_rows.append(to_row(slot, eye).astype(jnp.int32))
     expo = jnp.exp(logits_ref[...])
-    gw = to_col(gw_ref[...], eye)
-    total = expo[:, 0:1] + expo[:, 1:2]
-    gates = [gw * expo[:, k:k + 1] / total for k in range(2)]
-
-    for q in range(4):
-        nq[q * 128:(q + 1) * 128, :] = normed_ref[:, q * 512:(q + 1) * 512]
+    total = expo[0:1, :] + expo[1:2, :]
+    gates = [to_col(gw_ref[...] * expo[k:k + 1, :] / total, eye) for k in range(2)]
     m = iota((512, 512), 0)
     n = iota((512, 512), 1)
     fold[...] = (m == (n & 127) * 4 + (n >> 7)).astype(BF)
@@ -129,8 +144,68 @@
     def span(c):
         return pl.ds(16 if c == 0 else c * 512, 496 if c == 0 else 512)
 
+    pl.semaphore_wait(barrier, 127)
+    up, down = lax.rem(sp + 1, 64), lax.rem(sp + 63, 64)
+
+    def to_edge(source, target, n, there):
+        return pltpu.make_async_remote_copy(
+            src_ref=source, dst_ref=target, send_sem=esend.at[n], recv_sem=erecv.at[n],
+            device_id=(there, tp), device_id_type=MESH)
+
+    edges = [
+        to_edge(product.at[240:256], edge_prev, 0, up),
+        to_edge(product.at[0:16], edge_next, 1, down),
+        to_edge(docs_ref, docs_prev, 2, up),
+        to_edge(docs_ref, docs_next, 3, down),
+    ]
+    for copy in edges:
+        copy.start()
+
+    def to_twin(at, size, n):
+        return pltpu.make_async_remote_copy(
+            src_ref=mixed.at[pl.ds(pl.multiple_of((1 - tp) * 128 + at, 16), size)],
+            dst_ref=theirs.at[pl.ds(pl.multiple_of(at, 16), size)],
+            send_sem=tsend.at[n], recv_sem=trecv.at[n], device_id=(sp, 1 - tp), device_id_type=MESH)
+
+    early = to_twin(tp * 16, 112, 0)
+    early.start()
+    for copy in edges:
+        copy.wait()
+    zero = (iota((32, 1), 0) == 0) & (sp == 0)
+    before = jnp.where(row[:32] == 0, (docs_prev[:, 255:256].astype(F32) == doc[:32]).astype(F32), same_prev[:32])
+    before = jnp.where(zero, 0.0, before)
+    first = mix(0, 32, edge_prev[15:16, :].astype(F32), None, before, same_next[:32])
+    zero = (iota((32, 1), 0) == 31) & (sp == 63)
+    after = jnp.where(row[:32] == 31, (docs_next[:, 0:1].astype(F32) == doc[224:]).astype(F32), same_next[224:])
+    after = jnp.where(zero, 0.0, after)
+    last = mix(224, 32, None, edge_next[0:1, :].astype(F32), same_prev[224:], after)
+    mixed[0:16, :] = first[:16]
+    mixed[240:256, :] = last[16:]
+    late = to_twin((1 - tp) * 112, 16, 1)
+    late.start()
+
+    for load in loads[8:11]:
+        load.wait()
+    mine = pl.ds(pl.multiple_of(tp * 128, 128), 128)
+    near = pl.ds(pl.multiple_of(tp * 512, 512), 512)
+    far = pl.ds(pl.multiple_of((1 - tp) * 512, 512), 512)
+    for q in range(4):
+        cols = slice(q * 512, (q + 1) * 512)
+        resid[:, cols] = stream_ref[:, cols].astype(F32) + dot(mixed[mine, :], ow[near, cols])
+    early.wait()
+    late.wait()
+    square = jnp.zeros((128, 1), F32)
+    for q in range(4):
+        cols = slice(q * 512, (q + 1) * 512)
+        value = resid[:, cols] + dot(theirs[...], ow[far, cols])
+        resid[:, cols] = value
+        square += jnp.sum(value * value, axis=1, keepdims=True)
+    scale = lax.rsqrt(square / 2048.0 + 1e-06)
+    for q in range(4):
+        cols = slice(q * 512, (q + 1) * 512)
+        nq[q * 128:(q + 1) * 128, :] = (resid[:, cols] * scale * gain_ref[:, cols]).astype(BF)
+
     pack(0)
-    pl.semaphore_wait(barrier, 127)
     for c in range(CHUNKS):
         @pl.loop(max(1, c * PER), (c + 1) * PER)
         def _(k):
@@ -138,7 +213,7 @@
         if c + 1 < CHUNKS:
             pack(c + 1)
     inbox[0:16, :] = outbox[0:16, :]
-    for load in loads:
+    for load in loads[11:]:
         load.wait()
 
     for c in range(CHUNKS):
@@ -183,59 +258,50 @@
             else:
                 found = found + acc[:, cols]
                 out_ref[:, cols] = (
-                    resid_ref[:, cols] + (gates[0] * found[:128] + gates[1] * found[128:])).astype(BF)
+                    resid[:, cols] + (gates[0] * found[:128] + gates[1] * found[128:])).astype(BF)
     for c in range(CHUNKS):
         s = span(c)
         pltpu.make_async_copy(outbox.at[s], outbox.at[s], send1.at[c]).wait()
         pltpu.make_async_copy(outbox2.at[s], outbox2.at[s], send2.at[c]).wait()
 
 
-def experts(normed, resid, ids, logits, gw, w_gate, w_up, w_down):
+def on_device(
+    stream, outer_gate, inner_gate, conv_values, doc_ids, conv_taps, out_weight, norm_gain,
+    route_ids, route_logits, group_weight, w_gate, w_up, w_down,
+):
     vmem = pl.BlockSpec(memory_space=pltpu.VMEM)
-    hbm = pl.BlockSpec(memory_space=pl.ANY)
+    hbm = pl.BlockSpec(memory_space=pltpu.HBM)
     box = pltpu.VMEM((2048, 512), BF)
     sems = pltpu.SemaphoreType.DMA((CHUNKS,))
+    docs = pltpu.VMEM((1, 256), jnp.int32)
+    edge = pltpu.VMEM((16, 512), BF)
     return pl.pallas_call(
         kernel,
         out_shape=jax.ShapeDtypeStruct((128, 2048), BF),
-        in_specs=[vmem] * 5 + [hbm] * 3,
+        in_specs=[hbm] * 14,
         out_specs=vmem,
         scratch_shapes=[
+            pltpu.VMEM((256, 512), BF), pltpu.VMEM((256, 512), BF), docs, pltpu.VMEM((256, 512), BF),
+            pltpu.VMEM((3, 512), F32), pltpu.VMEM((2, 128), jnp.int32), pltpu.VMEM((2, 128), F32),
+            pltpu.VMEM((1, 128), F32), pltpu.VMEM((128, 2048), BF), pltpu.VMEM((1, 2048), F32),
+            pltpu.VMEM((1024, 2048), BF),
             pltpu.VMEM((2048, 1024), BF), pltpu.VMEM((2048, 1024), BF), pltpu.VMEM((1024, 2048), BF),
+            pltpu.VMEM((256, 512), BF), pltpu.VMEM((256, 512), BF), edge, edge, docs, docs,
+            pltpu.VMEM((128, 512), BF), pltpu.VMEM((128, 2048), F32),
             pltpu.VMEM((512, 512), BF), pltpu.VMEM((512, 512), BF), pltpu.VMEM((512, 512), BF),
             box, box, box, box,
             pltpu.VMEM((128, 2048), BF), pltpu.VMEM((128, 1024), BF), pltpu.VMEM((512, 512), BF),
             pltpu.VMEM((256, 2048), F32),
-            pltpu.SemaphoreType.DMA((3,)), sems, sems, sems, sems,
+            pltpu.SemaphoreType.DMA((14,)), pltpu.SemaphoreType.DMA((4,)), pltpu.SemaphoreType.DMA((4,)),
+            pltpu.SemaphoreType.DMA((2,)), pltpu.SemaphoreType.DMA((2,)), sems, sems, sems, sems,
         ],
         compiler_params=pltpu.CompilerParams(
-            collective_id=0, has_side_effects=True, vmem_limit_bytes=50 * 2**20),
-        name="experts",
-    )(normed, resid, ids, logits, gw, w_gate, w_up, w_down)
-
-
-def on_device(
-    stream, outer_gate, inner_gate, conv_values, doc_ids, conv_taps, out_weight, norm_gain,
-    route_ids, route_logits, group_weight, w_gate, w_up, w_down,
-):
-    product = (inner_gate.astype(F32) * conv_values.astype(F32)).astype(BF)
-    doc_float = doc_ids.astype(BF)
-    padded, padded_docs = (padded_2(product, (("sp", 0),), 1), padded_2(doc_float, (("sp", 0),), 1))
-    same_prev = (padded_docs[:-2] == doc_float).astype(F32)[:, None]
-    same_next = (padded_docs[2:] == doc_float).astype(F32)[:, None]
-    conv = (
-        conv_taps[0] * padded[:-2].astype(F32) * same_prev
-        + conv_taps[1] * product.astype(F32)
-        + conv_taps[2] * padded[2:].astype(F32) * same_next
-    )
-    mixed = (outer_gate.astype(F32) * conv).astype(BF)
-    channels = lax.all_to_all(mixed, "tp", split_axis=0, concat_axis=1, tiled=True)
-    projected = jnp.dot(channels, out_weight, preferred_element_type=F32)
-    resid = stream.astype(F32) + projected
-    scale = lax.rsqrt(jnp.mean(resid * resid, axis=-1, keepdims=True) + 1e-06)
-    normed = (resid * scale * norm_gain).astype(BF)
-    return experts(
-        normed, resid, route_ids, route_logits, group_weight.reshape(1, 128), w_gate, w_up, w_down)
+            collective_id=0, has_side_effects=True, vmem_limit_bytes=60 * 1024 * 1024),
+        name="layer",
+    )(
+        stream, outer_gate, inner_gate, conv_values, doc_ids.reshape(1, 256), conv_taps,
+        norm_gain.reshape(1, 2048), route_ids.T, route_logits.T, group_weight.reshape(1, 128),
+        out_weight, w_gate, w_up, w_down)
 
 
 def solution(mesh):

time: 103 us -> 73.3 us (0.71)
  the two profiles are of different devices: /device:TPU:19 before, /device:TPU:1 now
where the time goes in v2:
time: 73.3 us; the launch traced here: 72.7 us
  Pallas kernels  70.8 us (97%)
  local copies, waits for them, and re-layouts  1.88 us (3%)
    pallas_call x1, Pallas kernels, on_device(): pl.pallas_call(kernel, out_shape=jax.ShapeDtypeStruct((128, 2048), BF), i...  70.8 us
    unnamed x1, local copies, waits for them, and re-layouts  1.88 us

profile of v2, /device:TPU:1, one launch (start us, length us, event | category | flops | bytes accessed | tf_op | source)
XLA Modules:
  0.0 72.7 jit_solution(13180290459170125808)
XLA Ops:
  0.0 70.8 %layer.1 = bf16[128,2048]{1,0:T(8,128)(2,1)} custom-call(bf16[128,2048]{1,0:T(8,128)(2,1)} %stream_hbm.1, bf16[256,512]{1,0:T(8,128)(2,1)} %outer_hbm.1, bf16[256,512]{1,0:T(8,128)(2,1)} %inner_hbm.1, bf16[256,512]{1,0:T(8,128)(2,1)} %values_hbm.1, s32[1,256]{1,0:T(1,128)} %bitcast.6, f32[3,512]{1,0:T(4,128)} %taps_hbm.1, f32[1,2048]{1,0:T(1,128)} %bitcast.5, ...), custom_call_target="tpu_custom_call" | custom-call | tf_op jit(solution)/shard_map/layer/pallas_call | solution.py:278
  70.8 1.9 %copy.16 = bf16[128,2048]{1,0:T(8,128)(2,1)} copy(bf16[128,2048]{1,0:T(8,128)(2,1)} %layer.1) | data formatting | bytes 1048576

commit v3 on v2

--- a/solution.py
+++ b/solution.py
@@ -47,9 +47,9 @@
     ow_hbm, wg_hbm, wu_hbm, wd_hbm,
     out_ref,
     inner_ref, values_ref, docs_ref, outer_ref, taps_ref, ids_ref, logits_ref, gw_ref, stream_ref, gain_ref,
-    ow, wg, wu, wd, product, mixed, edge_prev, edge_next, docs_prev, docs_next, theirs, resid,
+    ow, wg, wu, wd, product, mixed, edge, twin_edge, my_edge, docs_near, theirs, resid,
     nq, fold, unfold, outbox, inbox, outbox2, inbox2, xbuf, hbuf, yq, acc,
-    wsem, esend, erecv, tsend, trecv, send1, recv1, send2, recv2,
+    wsem, row_sem, plane_sem, esend, erecv, tsend, trecv, send1, recv1, send2, recv2,
 ):
     sp, tp = lax.axis_index("sp"), lax.axis_index("tp")
     pairs = [
@@ -61,35 +61,82 @@
     loads = [pltpu.make_async_copy(a, b, wsem.at[i]) for i, (a, b) in enumerate(pairs)]
     for load in loads:
         load.start()
+    z, y, x = sp // 16, lax.rem(sp // 4, 4), lax.rem(sp, 4)
+
+    def spot(dz, dy, dx):
+        return lax.rem(z + dz, 4) * 16 + lax.rem(y + dy, 4) * 4 + lax.rem(x + dx, 4)
+
+    def signal(sem, there, core):
+        pl.semaphore_signal(sem, inc=1, device_id=(there, core), device_id_type=MESH)
+
     barrier = pltpu.get_barrier_semaphore()
-
-    @pl.loop(1, 128)
-    def _(k):
-        pl.semaphore_signal(barrier, inc=1, device_id=partner(k, 1, sp, tp), device_id_type=MESH)
-
-    for load in loads[:5]:
+    up, down = lax.rem(sp + 1, 64), lax.rem(sp + 63, 64)
+    beside = jnp.where(tp == 0, down, up)
+    for core in range(2):
+        signal(barrier, beside, core)
+    signal(barrier, sp, 1 - tp)
+    for d in range(1, 4):
+        for core in range(2):
+            signal(barrier, spot(0, 0, d), core)
+        signal(barrier, spot(0, d, 0), tp)
+        signal(barrier, spot(d, 0, 0), tp)
+
+    for load in loads[:3]:
         load.wait()
     product[...] = (inner_ref[...].astype(F32) * values_ref[...].astype(F32)).astype(BF)
+    pl.semaphore_wait(barrier, 15)
+    for d in range(1, 4):
+        signal(row_sem, spot(0, d, 0), tp)
+
+    def to_edge(source, target, n, m, there, core):
+        return pltpu.make_async_remote_copy(
+            src_ref=source, dst_ref=target, send_sem=esend.at[n], recv_sem=erecv.at[m],
+            device_id=(there, core), device_id_type=MESH)
+
+    edges = [
+        to_edge(product.at[240:256], edge.at[tp], 0, tp, up, 0),
+        to_edge(product.at[0:16], edge.at[tp], 1, tp, down, 1),
+        to_edge(docs_ref, docs_near, 2, 2, jnp.where(tp == 0, up, down), tp),
+    ]
+    for copy in edges:
+        copy.start()
+
+    for load in loads[3:5]:
+        load.wait()
     r0, r1 = iota((256, 256), 0), iota((256, 256), 1)
     docs = docs_ref[...].astype(F32)
     doc = to_col(docs, r0 == r1)
-    row = iota((256, 1), 0)
     same_prev = (to_col(docs, r0 == r1 + 1) == doc).astype(F32)
     same_next = (to_col(docs, r0 + 1 == r1) == doc).astype(F32)
-
-    def mix(lo, size, first, last, before, after):
-        rows = slice(lo, lo + size)
-        own = product[rows, :].astype(F32)
-        up, down = pltpu.roll(own, 1, 0), pltpu.roll(own, size - 1, 0)
-        at = iota((size, 1), 0)
-        if first is not None:
-            up = jnp.where(at == 0, first, up)
-        if last is not None:
-            down = jnp.where(at == size - 1, last, down)
-        conv = taps_ref[0:1, :] * up * before + taps_ref[1:2, :] * own + taps_ref[2:3, :] * down * after
-        return (outer_ref[rows, :].astype(F32) * conv).astype(BF)
-
-    mixed[...] = mix(0, 256, None, None, same_prev, same_next)
+    own = product[...].astype(F32)
+    outer = outer_ref[...].astype(F32)
+    tap = [taps_ref[k:k + 1, :] for k in range(3)]
+    conv = tap[0] * pltpu.roll(own, 1, 0) * same_prev + tap[1] * own + tap[2] * pltpu.roll(own, 255, 0) * same_next
+    mixed[...] = (outer * conv).astype(BF)
+    base = [
+        outer[0:1] * (tap[1] * own[0:1] + tap[2] * own[1:2] * same_next[0:1]),
+        outer[255:256] * (tap[1] * own[255:256] + tap[0] * own[254:255] * same_prev[255:256]),
+    ]
+    coef = [outer[0:1] * tap[0], outer[255:256] * tap[2]]
+    here = tp == 0
+    my_base, my_coef = jnp.where(here, base[0], base[1]), jnp.where(here, coef[0], coef[1])
+    my_edge[...] = jnp.where(
+        iota((8, 512), 0) == 0, jnp.where(here, base[1], base[0]), jnp.where(here, coef[1], coef[0]))
+
+    def to_twin(source, target, n):
+        return pltpu.make_async_remote_copy(
+            src_ref=source, dst_ref=target, send_sem=tsend.at[n], recv_sem=trecv.at[n],
+            device_id=(sp, 1 - tp), device_id_type=MESH)
+
+    twins = [
+        to_twin(mixed.at[pl.ds(pl.multiple_of((1 - tp) * 128, 128), 128)], theirs, 0),
+        to_twin(my_edge, twin_edge, 1),
+    ]
+    for copy in twins:
+        copy.start()
+    pl.semaphore_wait(row_sem, 3)
+    for d in range(1, 4):
+        signal(plane_sem, spot(d, 0, 0), tp)
 
     for load in loads[5:8]:
         load.wait()
@@ -99,7 +146,6 @@
     hot = [(ids[k] == lane).astype(F32) for k in range(2)]
     before = (iota((128, 128), 0) > lane).astype(BF)
     count = dot(before, (hot[0] + hot[1]).astype(BF))
-    z, y, x = sp // 16, lax.rem(sp // 4, 4), lax.rem(sp, 4)
     slots, slot_rows = [], []
     for k in range(2):
         e = ids[k]
@@ -144,60 +190,38 @@
     def span(c):
         return pl.ds(16 if c == 0 else c * 512, 496 if c == 0 else 512)
 
-    pl.semaphore_wait(barrier, 127)
-    up, down = lax.rem(sp + 1, 64), lax.rem(sp + 63, 64)
-
-    def to_edge(source, target, n, there):
-        return pltpu.make_async_remote_copy(
-            src_ref=source, dst_ref=target, send_sem=esend.at[n], recv_sem=erecv.at[n],
-            device_id=(there, tp), device_id_type=MESH)
-
-    edges = [
-        to_edge(product.at[240:256], edge_prev, 0, up),
-        to_edge(product.at[0:16], edge_next, 1, down),
-        to_edge(docs_ref, docs_prev, 2, up),
-        to_edge(docs_ref, docs_next, 3, down),
-    ]
     for copy in edges:
-        copy.start()
-
-    def to_twin(at, size, n):
-        return pltpu.make_async_remote_copy(
-            src_ref=mixed.at[pl.ds(pl.multiple_of((1 - tp) * 128 + at, 16), size)],
-            dst_ref=theirs.at[pl.ds(pl.multiple_of(at, 16), size)],
-            send_sem=tsend.at[n], recv_sem=trecv.at[n], device_id=(sp, 1 - tp), device_id_type=MESH)
-
-    early = to_twin(tp * 16, 112, 0)
-    early.start()
-    for copy in edges:
+        copy.wait_send()
+    for half in range(2):
+        to_edge(product.at[0:16], edge.at[half], 0, half, up, 0).wait_recv()
+    edges[2].wait_recv()
+    for copy in twins:
         copy.wait()
-    zero = (iota((32, 1), 0) == 0) & (sp == 0)
-    before = jnp.where(row[:32] == 0, (docs_prev[:, 255:256].astype(F32) == doc[:32]).astype(F32), same_prev[:32])
-    before = jnp.where(zero, 0.0, before)
-    first = mix(0, 32, edge_prev[15:16, :].astype(F32), None, before, same_next[:32])
-    zero = (iota((32, 1), 0) == 31) & (sp == 63)
-    after = jnp.where(row[:32] == 31, (docs_next[:, 0:1].astype(F32) == doc[224:]).astype(F32), same_next[224:])
-    after = jnp.where(zero, 0.0, after)
-    last = mix(224, 32, None, edge_next[0:1, :].astype(F32), same_prev[224:], after)
-    mixed[0:16, :] = first[:16]
-    mixed[240:256, :] = last[16:]
-    late = to_twin((1 - tp) * 112, 16, 1)
-    late.start()
+    beyond = jnp.where(here, docs_near[:, 255:256], docs_near[:, 0:1])
+    at_edge = jnp.where(here, docs_ref[:, 0:1], docs_ref[:, 255:256])
+    inside = jnp.where(here, sp > 0, sp < 63)
+    same = jnp.where((beyond == at_edge) & inside, 1.0, 0.0)
+
+    def place_edge(box, start, half, base_row, coef_row):
+        rows = pl.ds(pl.multiple_of(start + tp * 112, 16), 16)
+        block = edge[half].astype(F32)
+        near_row = jnp.where(here, block[15:16], block[0:1])
+        value = base_row + coef_row * near_row * same
+        box[rows, :] = jnp.where(iota((16, 512), 0) == tp * 15, value, box[rows, :].astype(F32)).astype(BF)
+
+    place_edge(mixed, tp * 128, tp, my_base, my_coef)
+    place_edge(theirs, 0, 1 - tp, twin_edge[0:1, :], twin_edge[1:2, :])
 
     for load in loads[8:11]:
         load.wait()
     mine = pl.ds(pl.multiple_of(tp * 128, 128), 128)
     near = pl.ds(pl.multiple_of(tp * 512, 512), 512)
     far = pl.ds(pl.multiple_of((1 - tp) * 512, 512), 512)
-    for q in range(4):
-        cols = slice(q * 512, (q + 1) * 512)
-        resid[:, cols] = stream_ref[:, cols].astype(F32) + dot(mixed[mine, :], ow[near, cols])
-    early.wait()
-    late.wait()
     square = jnp.zeros((128, 1), F32)
     for q in range(4):
         cols = slice(q * 512, (q + 1) * 512)
-        value = resid[:, cols] + dot(theirs[...], ow[far, cols])
+        value = stream_ref[:, cols].astype(F32) + (
+            dot(mixed[mine, :], ow[near, cols]) + dot(theirs[...], ow[far, cols]))
         resid[:, cols] = value
         square += jnp.sum(value * value, axis=1, keepdims=True)
     scale = lax.rsqrt(square / 2048.0 + 1e-06)
@@ -206,6 +230,7 @@
         nq[q * 128:(q + 1) * 128, :] = (resid[:, cols] * scale * gain_ref[:, cols]).astype(BF)
 
     pack(0)
+    pl.semaphore_wait(plane_sem, 3)
     for c in range(CHUNKS):
         @pl.loop(max(1, c * PER), (c + 1) * PER)
         def _(k):
@@ -274,7 +299,7 @@
     box = pltpu.VMEM((2048, 512), BF)
     sems = pltpu.SemaphoreType.DMA((CHUNKS,))
     docs = pltpu.VMEM((1, 256), jnp.int32)
-    edge = pltpu.VMEM((16, 512), BF)
+    edge = pltpu.VMEM((8, 512), F32)
     return pl.pallas_call(
         kernel,
         out_shape=jax.ShapeDtypeStruct((128, 2048), BF),
@@ -286,13 +311,14 @@
             pltpu.VMEM((1, 128), F32), pltpu.VMEM((128, 2048), BF), pltpu.VMEM((1, 2048), F32),
             pltpu.VMEM((1024, 2048), BF),
             pltpu.VMEM((2048, 1024), BF), pltpu.VMEM((2048, 1024), BF), pltpu.VMEM((1024, 2048), BF),
-            pltpu.VMEM((256, 512), BF), pltpu.VMEM((256, 512), BF), edge, edge, docs, docs,
+            pltpu.VMEM((256, 512), BF), pltpu.VMEM((256, 512), BF), pltpu.VMEM((2, 16, 512), BF), edge, edge, docs,
             pltpu.VMEM((128, 512), BF), pltpu.VMEM((128, 2048), F32),
             pltpu.VMEM((512, 512), BF), pltpu.VMEM((512, 512), BF), pltpu.VMEM((512, 512), BF),
             box, box, box, box,
             pltpu.VMEM((128, 2048), BF), pltpu.VMEM((128, 1024), BF), pltpu.VMEM((512, 512), BF),
             pltpu.VMEM((256, 2048), F32),
-            pltpu.SemaphoreType.DMA((14,)), pltpu.SemaphoreType.DMA((4,)), pltpu.SemaphoreType.DMA((4,)),
+            pltpu.SemaphoreType.DMA((14,)), pltpu.SemaphoreType.REGULAR, pltpu.SemaphoreType.REGULAR,
+            pltpu.SemaphoreType.DMA((3,)), pltpu.SemaphoreType.DMA((3,)),
             pltpu.SemaphoreType.DMA((2,)), pltpu.SemaphoreType.DMA((2,)), sems, sems, sems, sems,
         ],
         compiler_params=pltpu.CompilerParams(

time: 73.3 us -> 65.1 us (0.89)
  Pallas kernels: 70.8 us -> 63 us
    pallas_call x1, Pallas kernels: 70.8 us -> 63 us  [on_device(): pl.pallas_call(kernel, out_shape=jax.ShapeDtypeStruct((128, 2048), BF), i...]
where the time goes in v3:
time: 65.1 us; the launch traced here: 64.9 us
  Pallas kernels  63 us (97%)
  local copies, waits for them, and re-layouts  1.88 us (3%)
    pallas_call x1, Pallas kernels, on_device(): pl.pallas_call(kernel, out_shape=jax.ShapeDtypeStruct((128, 2048), BF), i...  63 us
    unnamed x1, local copies, waits for them, and re-layouts  1.88 us

profile of v3, /device:TPU:1, one launch (start us, length us, event | category | flops | bytes accessed | tf_op | source)
XLA Modules:
  0.0 64.9 jit_solution(6675567880966896204)
XLA Ops:
  0.0 63.0 %layer.1 = bf16[128,2048]{1,0:T(8,128)(2,1)} custom-call(bf16[128,2048]{1,0:T(8,128)(2,1)} %stream_hbm.1, bf16[256,512]{1,0:T(8,128)(2,1)} %outer_hbm.1, bf16[256,512]{1,0:T(8,128)(2,1)} %inner_hbm.1, bf16[256,512]{1,0:T(8,128)(2,1)} %values_hbm.1, s32[1,256]{1,0:T(1,128)} %bitcast.6, f32[3,512]{1,0:T(4,128)} %taps_hbm.1, f32[1,2048]{1,0:T(1,128)} %bitcast.5, ...), custom_call_target="tpu_custom_call" | custom-call | tf_op jit(solution)/shard_map/layer/pallas_call | solution.py:303
  63.0 1.9 %copy.16 = bf16[128,2048]{1,0:T(8,128)(2,1)} copy(bf16[128,2048]{1,0:T(8,128)(2,1)} %layer.1) | data formatting | bytes 1048576

commit v4 on v3

--- a/solution.py
+++ b/solution.py
@@ -8,10 +8,11 @@
 from jax.sharding import PartitionSpec as P
 
 MESH = pl.DeviceIdType.MESH
-STEP = 37
+STEP = 59
 BACK = pow(STEP, -1, 128)
-CHUNKS = 4
-PER = 32
+SIZES = (32, 32, 32, 32)
+CHUNKS = len(SIZES)
+STARTS = [sum(SIZES[:c]) for c in range(CHUNKS)]
 F32 = jnp.float32
 BF = jnp.bfloat16
 
@@ -59,7 +60,7 @@
         (wg_hbm.at[0], wg), (wu_hbm.at[0], wu), (wd_hbm.at[0], wd),
     ]
     loads = [pltpu.make_async_copy(a, b, wsem.at[i]) for i, (a, b) in enumerate(pairs)]
-    for load in loads:
+    for load in loads[:11]:
         load.start()
     z, y, x = sp // 16, lax.rem(sp // 4, 4), lax.rem(sp, 4)
 
@@ -162,10 +163,6 @@
     expo = jnp.exp(logits_ref[...])
     total = expo[0:1, :] + expo[1:2, :]
     gates = [to_col(gw_ref[...] * expo[k:k + 1, :] / total, eye) for k in range(2)]
-    m = iota((512, 512), 0)
-    n = iota((512, 512), 1)
-    fold[...] = (m == (n & 127) * 4 + (n >> 7)).astype(BF)
-    unfold[...] = (n == (m & 127) * 4 + (m >> 7)).astype(BF)
 
     def copy_out(k, c):
         rows = pl.ds(pl.multiple_of(k * 16, 16), 16)
@@ -180,15 +177,16 @@
             device_id=partner(k, -1, sp, tp), device_id_type=MESH)
 
     def pack(c):
-        base = c * 512
-        at = iota((512, 128), 0) + base
+        base, size = STARTS[c] * 16, SIZES[c] * 16
+        at = iota((size, 128), 0) + base
         mine = ((at >> 2) == slot_rows[0]) | ((at >> 2) == slot_rows[1])
         picks = [(mine & ((at & 3) == q)).astype(BF) for q in range(4)]
         packed = dot(jnp.concatenate(picks, axis=1), nq[...])
-        outbox[base:base + 512, :] = packed.astype(BF)
+        outbox[base:base + size, :] = packed.astype(BF)
 
     def span(c):
-        return pl.ds(16 if c == 0 else c * 512, 496 if c == 0 else 512)
+        first = max(1, STARTS[c])
+        return pl.ds(first * 16, (STARTS[c] + SIZES[c] - first) * 16)
 
     for copy in edges:
         copy.wait_send()
@@ -214,6 +212,8 @@
 
     for load in loads[8:11]:
         load.wait()
+    for load in loads[11:]:
+        load.start()
     mine = pl.ds(pl.multiple_of(tp * 128, 128), 128)
     near = pl.ds(pl.multiple_of(tp * 512, 512), 512)
     far = pl.ds(pl.multiple_of((1 - tp) * 512, 512), 512)
@@ -232,38 +232,43 @@
     pack(0)
     pl.semaphore_wait(plane_sem, 3)
     for c in range(CHUNKS):
-        @pl.loop(max(1, c * PER), (c + 1) * PER)
+        @pl.loop(max(1, STARTS[c]), STARTS[c] + SIZES[c])
         def _(k):
             copy_out(k, c).start()
         if c + 1 < CHUNKS:
             pack(c + 1)
     inbox[0:16, :] = outbox[0:16, :]
+    m = iota((512, 512), 0)
+    n = iota((512, 512), 1)
+    fold[...] = (m == (n & 127) * 4 + (n >> 7)).astype(BF)
+    unfold[...] = (n == (m & 127) * 4 + (m >> 7)).astype(BF)
     for load in loads[11:]:
         load.wait()
 
     for c in range(CHUNKS):
         s = span(c)
         pltpu.make_async_copy(inbox.at[s], inbox.at[s], recv1.at[c]).wait()
+        box = slice(STARTS[c] * 16, (STARTS[c] + SIZES[c]) * 16)
+        rows, size = SIZES[c] * 4, SIZES[c] * 16
         for q in range(4):
-            xq = dot(unfold[q * 128:(q + 1) * 128, :], inbox[c * 512:(c + 1) * 512, :])
-            xbuf[:, q * 512:(q + 1) * 512] = xq.astype(BF)
+            xq = dot(unfold[q * 128:q * 128 + rows, :size], inbox[box, :])
+            xbuf[:rows, q * 512:(q + 1) * 512] = xq.astype(BF)
 
         @pl.loop(0, 4)
         def _(n):
             cols = pl.ds(pl.multiple_of(n * 256, 256), 256)
-            g = dot(xbuf[...], wg[:, cols])
-            u = dot(xbuf[...], wu[:, cols])
-            hbuf[:, cols] = (g / (1.0 + jnp.exp(-g)) * u).astype(BF)
+            g = dot(xbuf[:rows, :], wg[:, cols])
+            u = dot(xbuf[:rows, :], wu[:, cols])
+            hbuf[:rows, cols] = (g / (1.0 + jnp.exp(-g)) * u).astype(BF)
 
         @pl.loop(0, 4)
         def _(q):
             cols = pl.ds(pl.multiple_of(q * 512, 512), 512)
-            rows = pl.ds(pl.multiple_of(q * 128, 128), 128)
-            yq[rows, :] = dot(hbuf[...], wd[:, cols]).astype(BF)
-
-        outbox2[c * 512:(c + 1) * 512, :] = dot(fold[...], yq[...]).astype(BF)
-
-        @pl.loop(max(1, c * PER), (c + 1) * PER)
+            yq[pl.ds(pl.multiple_of(q * 128, 128), rows), :] = dot(hbuf[:rows, :], wd[:, cols]).astype(BF)
+
+        outbox2[box, :] = dot(fold[:size, :], yq[...]).astype(BF)
+
+        @pl.loop(max(1, STARTS[c]), STARTS[c] + SIZES[c])
         def _(k):
             copy_back(k, c).start()
     inbox2[0:16, :] = outbox2[0:16, :]
@@ -271,11 +276,12 @@
     for c in range(CHUNKS):
         s = span(c)
         pltpu.make_async_copy(inbox2.at[s], inbox2.at[s], recv2.at[c]).wait()
-        at = iota((128, 512), 1) + c * 512
+        box = slice(STARTS[c] * 16, (STARTS[c] + SIZES[c]) * 16)
+        at = iota((128, SIZES[c] * 16), 1) + STARTS[c] * 16
         for q in range(4):
             cols = slice(q * 512, (q + 1) * 512)
             pick = jnp.concatenate([(at == slots[k] * 4 + q).astype(BF) for k in range(2)], axis=0)
-            found = dot(pick, inbox2[c * 512:(c + 1) * 512, :])
+            found = dot(pick, inbox2[box, :])
             if c == 0:
                 acc[:, cols] = found
             elif c + 1 < CHUNKS:
@@ -322,12 +328,12 @@
             pltpu.SemaphoreType.DMA((2,)), pltpu.SemaphoreType.DMA((2,)), sems, sems, sems, sems,
         ],
         compiler_params=pltpu.CompilerParams(
-            collective_id=0, has_side_effects=True, vmem_limit_bytes=60 * 1024 * 1024),
+            collective_id=0, has_side_effects=True, vmem_limit_bytes=44 * 2**20),
         name="layer",
-    )(
+    )(*[pltpu.with_memory_space_constraint(a, pltpu.HBM) for a in (
         stream, outer_gate, inner_gate, conv_values, doc_ids.reshape(1, 256), conv_taps,
         norm_gain.reshape(1, 2048), route_ids.T, route_logits.T, group_weight.reshape(1, 128),
-        out_weight, w_gate, w_up, w_down)
+        out_weight, w_gate, w_up, w_down)])
 
 
 def solution(mesh):

time: 65.1 us -> 62.9 us (0.966)
  local copies, waits for them, and re-layouts: 1.88 us -> 0.8 us
  Pallas kernels: 63 us -> 62 us
    unnamed x1, local copies, waits for them, and re-layouts: 1.88 us -> 0.8 us
    pallas_call x1, Pallas kernels: 63 us -> 62 us  [on_device(): pl.pallas_call(kernel, out_shape=jax.ShapeDtypeStruct((128, 2048), BF), i...]
where the time goes in v4:
time: 62.9 us; the launch traced here: 62.8 us
  Pallas kernels  62 us (99%)
  local copies, waits for them, and re-layouts  0.8 us (1%)
    pallas_call x1, Pallas kernels, on_device(): pl.pallas_call(kernel, out_shape=jax.ShapeDtypeStruct((128, 2048), BF), i...  62 us

profile of v4, /device:TPU:1, one launch (start us, length us, event | category | flops | bytes accessed | tf_op | source)
XLA Modules:
  0.0 62.8 jit_solution(10650274344254397712)
XLA Ops:
  0.0 62.0 %layer.1 = bf16[128,2048]{1,0:T(8,128)(2,1)S(1)} custom-call(bf16[128,2048]{1,0:T(8,128)(2,1)} %stream_hbm.1, bf16[256,512]{1,0:T(8,128)(2,1)} %outer_hbm.1, bf16[256,512]{1,0:T(8,128)(2,1)} %inner_hbm.1, bf16[256,512]{1,0:T(8,128)(2,1)} %values_hbm.1, s32[1,256]{1,0:T(1,128)} %bitcast.6, f32[3,512]{1,0:T(4,128)} %taps_hbm.1, f32[1,2048]{1,0:T(1,128)} %bitcast.5, ...), custom_call_target="tpu_custom_call" | custom-call | tf_op jit(solution)/shard_map/layer/pallas_call | solution.py:309
  62.0 0.8 %copy.16 = bf16[128,2048]{1,0:T(8,128)(2,1)} copy(bf16[128,2048]{1,0:T(8,128)(2,1)S(1)} %layer.1) | data formatting | bytes 1048576

commit v5 on v4

--- a/solution.py
+++ b/solution.py
@@ -49,7 +49,7 @@
     out_ref,
     inner_ref, values_ref, docs_ref, outer_ref, taps_ref, ids_ref, logits_ref, gw_ref, stream_ref, gain_ref,
     ow, wg, wu, wd, product, mixed, edge, twin_edge, my_edge, docs_near, theirs, resid,
-    nq, fold, unfold, outbox, inbox, outbox2, inbox2, xbuf, hbuf, yq, acc,
+    nq, fold, unfold, outbox, inbox, outbox2, inbox2, xbuf, hbuf, yq, acc, masks,
     wsem, row_sem, plane_sem, esend, erecv, tsend, trecv, send1, recv1, send2, recv2,
 ):
     sp, tp = lax.axis_index("sp"), lax.axis_index("tp")
@@ -176,18 +176,25 @@
             src_ref=outbox2.at[rows], dst_ref=inbox2.at[rows], send_sem=send2.at[c], recv_sem=recv2.at[c],
             device_id=partner(k, -1, sp, tp), device_id_type=MESH)
 
-    def pack(c):
+    def mask(c):
         base, size = STARTS[c] * 16, SIZES[c] * 16
         at = iota((size, 128), 0) + base
         mine = ((at >> 2) == slot_rows[0]) | ((at >> 2) == slot_rows[1])
-        picks = [(mine & ((at & 3) == q)).astype(BF) for q in range(4)]
-        packed = dot(jnp.concatenate(picks, axis=1), nq[...])
-        outbox[base:base + size, :] = packed.astype(BF)
+        return jnp.concatenate([(mine & ((at & 3) == q)).astype(BF) for q in range(4)], axis=1)
+
+    def pack(c, chosen):
+        base, size = STARTS[c] * 16, SIZES[c] * 16
+        outbox[base:base + size, :] = dot(chosen, nq[...]).astype(BF)
+
+    def picks(c, q):
+        at = iota((128, SIZES[c] * 16), 1) + STARTS[c] * 16
+        return jnp.concatenate([(at == slots[k] * 4 + q).astype(BF) for k in range(2)], axis=0)
 
     def span(c):
         first = max(1, STARTS[c])
         return pl.ds(first * 16, (STARTS[c] + SIZES[c] - first) * 16)
 
+    masks[:512, :] = mask(0)
     for copy in edges:
         copy.wait_send()
     for half in range(2):
@@ -229,14 +236,14 @@
         cols = slice(q * 512, (q + 1) * 512)
         nq[q * 128:(q + 1) * 128, :] = (resid[:, cols] * scale * gain_ref[:, cols]).astype(BF)
 
-    pack(0)
+    pack(0, masks[:512, :])
     pl.semaphore_wait(plane_sem, 3)
     for c in range(CHUNKS):
         @pl.loop(max(1, STARTS[c]), STARTS[c] + SIZES[c])
         def _(k):
             copy_out(k, c).start()
         if c + 1 < CHUNKS:
-            pack(c + 1)
+            pack(c + 1, mask(c + 1))
     inbox[0:16, :] = outbox[0:16, :]
     m = iota((512, 512), 0)
     n = iota((512, 512), 1)
@@ -275,12 +282,15 @@
 
     for c in range(CHUNKS):
         s = span(c)
+        final = c + 1 == CHUNKS
+        if final:
+            for q in range(4):
+                masks[q * 256:(q + 1) * 256, :] = picks(c, q)
         pltpu.make_async_copy(inbox2.at[s], inbox2.at[s], recv2.at[c]).wait()
         box = slice(STARTS[c] * 16, (STARTS[c] + SIZES[c]) * 16)
-        at = iota((128, SIZES[c] * 16), 1) + STARTS[c] * 16
         for q in range(4):
             cols = slice(q * 512, (q + 1) * 512)
-            pick = jnp.concatenate([(at == slots[k] * 4 + q).astype(BF) for k in range(2)], axis=0)
+            pick = masks[q * 256:(q + 1) * 256, :] if final else picks(c, q)
             found = dot(pick, inbox2[box, :])
             if c == 0:
                 acc[:, cols] = found
@@ -322,7 +332,7 @@
             pltpu.VMEM((512, 512), BF), pltpu.VMEM((512, 512), BF), pltpu.VMEM((512, 512), BF),
             box, box, box, box,
             pltpu.VMEM((128, 2048), BF), pltpu.VMEM((128, 1024), BF), pltpu.VMEM((512, 512), BF),
-            pltpu.VMEM((256, 2048), F32),
+            pltpu.VMEM((256, 2048), F32), pltpu.VMEM((1024, 512), BF),
             pltpu.SemaphoreType.DMA((14,)), pltpu.SemaphoreType.REGULAR, pltpu.SemaphoreType.REGULAR,
             pltpu.SemaphoreType.DMA((3,)), pltpu.SemaphoreType.DMA((3,)),
             pltpu.SemaphoreType.DMA((2,)), pltpu.SemaphoreType.DMA((2,)), sems, sems, sems, sems,

time: 62.9 us -> 63.8 us (1.014)
  Pallas kernels: 62 us -> 62.9 us
    pallas_call x1, Pallas kernels: 62 us -> 62.9 us  [on_device(): pl.pallas_call(kernel, out_shape=jax.ShapeDtypeStruct((128, 2048), BF), i...]
where the time goes in v5:
time: 63.8 us; the launch traced here: 63.7 us
  Pallas kernels  62.9 us (99%)
  local copies, waits for them, and re-layouts  0.8 us (1%)
    pallas_call x1, Pallas kernels, on_device(): pl.pallas_call(kernel, out_shape=jax.ShapeDtypeStruct((128, 2048), BF), i...  62.9 us

profile of v5, /device:TPU:1, one launch (start us, length us, event | category | flops | bytes accessed | tf_op | source)
XLA Modules:
  0.0 63.7 jit_solution(399439715461366453)
XLA Ops:
  0.0 62.9 %layer.1 = bf16[128,2048]{1,0:T(8,128)(2,1)S(1)} custom-call(bf16[128,2048]{1,0:T(8,128)(2,1)} %stream_hbm.1, bf16[256,512]{1,0:T(8,128)(2,1)} %outer_hbm.1, bf16[256,512]{1,0:T(8,128)(2,1)} %inner_hbm.1, bf16[256,512]{1,0:T(8,128)(2,1)} %values_hbm.1, s32[1,256]{1,0:T(1,128)} %bitcast.6, f32[3,512]{1,0:T(4,128)} %taps_hbm.1, f32[1,2048]{1,0:T(1,128)} %bitcast.5, ...), custom_call_target="tpu_custom_call" | custom-call | tf_op jit(solution)/shard_map/layer/pallas_call | solution.py:319
  62.9 0.8 %copy.16 = bf16[128,2048]{1,0:T(8,128)(2,1)} copy(bf16[128,2048]{1,0:T(8,128)(2,1)S(1)} %layer.1) | data formatting | bytes 1048576

commit v6 on v5

--- a/solution.py
+++ b/solution.py
@@ -194,7 +194,6 @@
         first = max(1, STARTS[c])
         return pl.ds(first * 16, (STARTS[c] + SIZES[c] - first) * 16)
 
-    masks[:512, :] = mask(0)
     for copy in edges:
         copy.wait_send()
     for half in range(2):
@@ -236,7 +235,7 @@
         cols = slice(q * 512, (q + 1) * 512)
         nq[q * 128:(q + 1) * 128, :] = (resid[:, cols] * scale * gain_ref[:, cols]).astype(BF)
 
-    pack(0, masks[:512, :])
+    pack(0, mask(0))
     pl.semaphore_wait(plane_sem, 3)
     for c in range(CHUNKS):
         @pl.loop(max(1, STARTS[c]), STARTS[c] + SIZES[c])

time: 63.8 us -> 62.9 us (0.986)
  Pallas kernels: 62.9 us -> 62 us
    pallas_call x1, Pallas kernels: 62.9 us -> 62 us  [on_device(): pl.pallas_call(kernel, out_shape=jax.ShapeDtypeStruct((128, 2048), BF), i...]
where the time goes in v6:
time: 62.9 us; the launch traced here: 62.8 us
  Pallas kernels  62 us (99%)
  local copies, waits for them, and re-layouts  0.8 us (1%)
    pallas_call x1, Pallas kernels, on_device(): pl.pallas_call(kernel, out_shape=jax.ShapeDtypeStruct((128, 2048), BF), i...  62 us

profile of v6, /device:TPU:1, one launch (start us, length us, event | category | flops | bytes accessed | tf_op | source)
XLA Modules:
  0.0 62.8 jit_solution(14645085422841417746)
XLA Ops:
  0.0 62.0 %layer.1 = bf16[128,2048]{1,0:T(8,128)(2,1)S(1)} custom-call(bf16[128,2048]{1,0:T(8,128)(2,1)} %stream_hbm.1, bf16[256,512]{1,0:T(8,128)(2,1)} %outer_hbm.1, bf16[256,512]{1,0:T(8,128)(2,1)} %inner_hbm.1, bf16[256,512]{1,0:T(8,128)(2,1)} %values_hbm.1, s32[1,256]{1,0:T(1,128)} %bitcast.6, f32[3,512]{1,0:T(4,128)} %taps_hbm.1, f32[1,2048]{1,0:T(1,128)} %bitcast.5, ...), custom_call_target="tpu_custom_call" | custom-call | tf_op jit(solution)/shard_map/layer/pallas_call | solution.py:318
  62.0 0.8 %copy.16 = bf16[128,2048]{1,0:T(8,128)(2,1)} copy(bf16[128,2048]{1,0:T(8,128)(2,1)S(1)} %layer.1) | data formatting | bytes 1048576
